TPU v7x, 32 devices: a whole 2x2x4 slice. The times are simulated.
32 devices in a mesh: ep: 8 (over z, core), tp: 4 (over y, x).
Axes of the slice: x: 2, y: 2, z: 4, core: 2. Of those that a mesh axis runs over, the one named last changes fastest.
Arguments:
- tokens: bfloat16 [512, 4096], P('ep', 'tp'), may hold values from -600 to 600
- in_gain: float32 [4096], P('tp'), may hold values from 0.1 to 1.9
- out_gain: float32 [4096], P('tp'), may hold values from 0.1 to 1.9
- routes: int32 [512, 4], replicated, may hold values from 0 to 31, as said below
- route_weights: float32 [512, 4], replicated, may hold values from 0.05 to 1
- w_gate: bfloat16 [32, 4096, 1024], P('ep', 'tp'), may hold values from -0.09375 to 0.09375
- w_up: bfloat16 [32, 4096, 1024], P('ep', 'tp'), may hold values from -0.09375 to 0.09375
- w_down: bfloat16 [32, 1024, 4096], P('ep', None, 'tp'), may hold values from -0.375 to 0.375
Outputs:
- result: bfloat16 [512, 4096], P('ep', 'tp')
Inputs may be any that keep to these rules, and one draw needn't show every extreme that they name: `routes`: each row names 4 different experts, all in one group of 8 consecutive numbers. In the rows of one index of ep (aligned blocks of 64 rows) no expert is named by more than 16 rows, and some expert by exactly 16.
All inputs are finite; a program needn't handle non-finite values.
Results may differ from a plain program's by a relative error of at most 0.025.
Values may be sent and summed in bfloat16 or wider, within the bound.
A program may use at most 64 MiB of HBM per device.

v0:
```python
import jax
import jax.numpy as jnp
from jax import lax
from jax.sharding import PartitionSpec as P

D = 4096
EPS = 1e-06


def run_experts(slot_rows, w_gate, w_up, w_down):
    gate_part = jnp.einsum(
        "secd,edf->secf", slot_rows, w_gate, preferred_element_type=jnp.float32
    ).astype(jnp.bfloat16)
    up_part = jnp.einsum(
        "secd,edf->secf", slot_rows, w_up, preferred_element_type=jnp.float32
    ).astype(jnp.bfloat16)
    gate_sum, up_sum = (
        lax.psum(gate_part, "tp").astype(jnp.float32),
        lax.psum(up_part, "tp").astype(jnp.float32),
    )
    active = (jax.nn.silu(gate_sum) * up_sum).astype(jnp.bfloat16)
    return jnp.einsum("secf,efd->secd", active, w_down, preferred_element_type=jnp.float32).astype(
        jnp.bfloat16
    )


def on_device(tokens, in_gain, out_gain, routes, route_weights, w_gate, w_up, w_down):
    tok_rows, local_width = tokens.shape
    top_count = routes.shape[1]
    local_experts = w_gate.shape[0]
    groups_ep = lax.axis_size("ep")
    experts = local_experts * groups_ep
    capacity = max(2, 2 * tok_rows * top_count // experts)
    values = tokens.astype(jnp.float32)
    sum_squares = lax.psum(jnp.sum(values * values, axis=1), "tp")
    normed = (values * lax.rsqrt(sum_squares / D + EPS)[:, None] * in_gain).astype(jnp.bfloat16)
    row_start = lax.axis_index("ep") * tok_rows
    my_routes = lax.dynamic_slice_in_dim(routes, row_start, tok_rows, 0)
    my_weights = lax.dynamic_slice_in_dim(route_weights, row_start, tok_rows, 0)
    flat_ids = my_routes.reshape(-1)
    matches = (flat_ids[:, None] == jnp.arange(experts, dtype=jnp.int32)[None, :]).astype(jnp.int32)
    slot_rank = jnp.sum((jnp.cumsum(matches, axis=0) - matches) * matches, axis=1)
    position = flat_ids * capacity + slot_rank
    dispatch_table = jnp.any(
        position.reshape(tok_rows, top_count, 1)
        == jnp.arange(experts * capacity, dtype=jnp.int32)[None, None, :],
        axis=1,
    )
    outgoing = jnp.einsum(
        "ts,td->sd", dispatch_table.astype(jnp.bfloat16), normed, preferred_element_type=jnp.float32
    ).astype(jnp.bfloat16)
    outgoing = outgoing.reshape(groups_ep, local_experts, capacity, local_width)
    answers = run_experts(
        lax.all_to_all(outgoing, "ep", split_axis=0, concat_axis=0, tiled=True),
        w_gate,
        w_up,
        w_down,
    )
    returned = lax.all_to_all(answers, "ep", split_axis=0, concat_axis=0, tiled=True)
    flat_out = returned.reshape(experts * capacity, local_width)
    picked = flat_out[position].reshape(tok_rows, top_count, local_width)
    combined = jnp.sum(my_weights[:, :, None] * picked.astype(jnp.float32), axis=1)
    out_squares = lax.psum(jnp.sum(combined * combined, axis=1), "tp")
    return (combined * lax.rsqrt(out_squares / D + EPS)[:, None] * out_gain).astype(jnp.bfloat16)


def solution(mesh):
    placed = (
        P("ep", "tp"),
        P("tp"),
        P("tp"),
        P(),
        P(),
        P("ep", "tp", None),
        P("ep", "tp", None),
        P("ep", None, "tp"),
    )
    return jax.shard_map(
        on_device, mesh=mesh, in_specs=placed, out_specs=P("ep", "tp"), check_vma=False
    )
```

profile of v0, /device:TPU:0, one launch (start us, length us, event | category | flops | bytes accessed | tf_op | source)
XLA Modules:
  0.0 185.9 jit_solution(116999732136430107)
XLA Ops:
  6.5 0.0 copy-start
  6.5 0.0 all-reduce.3.cloned.1.call-start
  6.5 0.7 copy-done
  7.2 0.1 constant_dynamic-slice_fusion
  7.3 0.1 copy.33
  7.4 0.1 eq.42
  7.5 0.1 eq.38
  7.6 0.6 reduce-window.6
  8.2 0.2 slice_reduce_fusion
  8.5 0.1 fusion.42
  8.6 0.1 reduce_sum.41
  8.7 0.1 copy.26
  8.8 0.1 fusion.33
  8.9 1.0 fusion.34
  10.0 11.4 %psum.28 = f32[64]{0:T(128)S(1)} all-reduce(f32[64]{0:T(128)S(1)} %fusion.34), channel_id=1, replica_groups=mesh['ep'=8,'tp'=4] {'tp'}, use_global_device_ids=true, to_apply=%region_5.6 | all-reduce | flops 64 | bytes 512 | tf_op jit(solution)/shard_map/psum | solution.py:35
  21.4 1.4 convolution_convert_fusion
  22.8 31.2 %all_to_all.10 = bf16[8,4,16,1024]{3,2,1,0:T(8,128)(2,1)S(1)} all-to-all(bf16[8,4,16,1024]{3,2,1,0:T(8,128)(2,1)S(1)} %bitcast.58), channel_id=1, replica_groups=mesh['ep'=8,'tp'=4] {'ep'}, dimensions={0} | all-to-all | bytes 2097152 | tf_op jit(solution)/shard_map/all_to_all | solution.py:54
  54.0 0.0 copy-start.1
  54.0 5.9 %fusion.23 = bf16[8,4,16,1024]{3,2,0,1:T(8,128)(2,1)} fusion(bf16[4,1024,1024]{2,1,0:T(8,128)(2,1)} %param.14, bf16[8,4,16,1024]{3,2,1,0:T(8,128)(2,1)S(1)} %all_to_all.10), kind=kOutput, calls=%fused_computation.19 | convolution fusion | flops 1074266112 | bytes 10485760 | tf_op jit(solution)/shard_map/secd,edf->secf/dot_general | solution.py:14
  59.9 0.0 copy-done.1
  59.9 2.3 %fusion.26 = bf16[8,4,16,1024]{3,2,0,1:T(8,128)(2,1)} fusion(bf16[4,1024,1024]{2,1,0:T(8,128)(2,1)S(1)} %copy-done.1, bf16[8,4,16,1024]{3,2,1,0:T(8,128)(2,1)S(1)} %all_to_all.10), kind=kOutput, calls=%fused_computation.20 | convolution fusion | flops 1074266112 | bytes 10485760 | tf_op jit(solution)/shard_map/secd,edf->secf/dot_general | solution.py:11
  62.1 0.0 all-reduce.3.cloned.1.call-update
  62.2 66.7 %all-reduce.3.cloned.1.call-done = (bf16[8,4,16,1024]{3,2,0,1:T(8,128)(2,1)}, bf16[8,4,16,1024]{3,2,0,1:T(8,128)(2,1)}) async-done(((bf16[8,4,16,1024]{3,2,0,1:T(8,128)(2,1)}, bf16[8,4,16,1024]{3,2,0,1:T(8,128)(2,1)}), (bf16[8,4,16,1024]{3,2,0,1:T(8,128)(2,1)}, bf16[8,4,16,1024]{3,2,0,1:T(8,128)(2,1)})) %all-reduce.3.cloned.1.call-update) | async-done | bytes 2097168 | tf_op jit(solution)/shard_map/psum | solution.py:19
  128.9 5.9 %fusion.20 = bf16[8,4,16,1024]{3,2,0,1:T(8,128)(2,1)S(1)} fusion(bf16[4,1024,1024]{2,1,0:T(8,128)(2,1)} %param.15, bf16[8,4,16,1024]{3,2,0,1:T(8,128)(2,1)} %get-tuple-element.5, bf16[8,4,16,1024]{3,2,0,1:T(8,128)(2,1)} %get-tuple-element.6), kind=kOutput, calls=%fused_computation.18 | convolution fusion | flops 1078460416 | bytes 11534336 | tf_op jit(solution)/shard_map/secf,efd->secd/dot_general | solution.py:22
  134.8 1.1 copy.29
  135.9 4.6 %all-to-all-start.1 = ((bf16[8,4,16,1024]{3,2,1,0:T(8,128)(2,1)}), bf16[8,4,16,1024]{3,2,1,0:T(8,128)(2,1)S(1)}, u32[]{:S(2)}, u32[]{:S(2)}) async-start(bf16[8,4,16,1024]{3,2,1,0:T(8,128)(2,1)} %copy.29), calls=%async_computation.1 | async-start | bytes 2097152 | tf_op jit(solution)/shard_map/all_to_all | solution.py:59
  140.5 0.1 mul.89
  140.6 0.8 constant_dynamic-slice_fusion.1
  141.3 0.1 copy.23
  141.5 25.6 %all-to-all-done.1 = bf16[8,4,16,1024]{3,2,1,0:T(8,128)(2,1)S(1)} async-done(((bf16[8,4,16,1024]{3,2,1,0:T(8,128)(2,1)}), bf16[8,4,16,1024]{3,2,1,0:T(8,128)(2,1)S(1)}, u32[]{:S(2)}, u32[]{:S(2)}) %all-to-all-start.1) | async-done | bytes 1048608 | tf_op jit(solution)/shard_map/all_to_all | solution.py:59
  167.0 1.2 gather_fusion
  168.2 0.0 copy-start.2
  168.2 0.3 reshape.70
  168.6 0.7 multiply_reduce_fusion
  169.3 0.1 multiply_reduce_fusion.1
  169.4 8.9 %psum.31 = f32[64]{0:T(128)S(1)} all-reduce(f32[64]{0:T(128)S(1)} %multiply_reduce_fusion.1), channel_id=1, replica_groups=mesh['ep'=8,'tp'=4] {'tp'}, use_global_device_ids=true, to_apply=%region_10.11 | all-reduce | flops 64 | bytes 512 | tf_op jit(solution)/shard_map/psum | solution.py:63
  178.3 0.0 copy-done.2
  178.3 0.8 multiply_convert_fusion
  (8 shorter events, 0.1 us)
Async XLA Ops:
  6.5 0.7 copy-start
  6.5 122.3 %all-reduce.3.cloned.1.call-start = ((), (), s32[]{:S(2)}) async-start(), calls=%async_computation.2 | async-start | bytes 4194304 | tf_op jit(solution)/shard_map/psum | solution.py:19
  54.0 5.9 %copy-start.1 = (bf16[4,1024,1024]{2,1,0:T(8,128)(2,1)S(1)}, bf16[4,1024,1024]{2,1,0:T(8,128)(2,1)}, u32[]{:S(2)}) copy-start(bf16[4,1024,1024]{2,1,0:T(8,128)(2,1)} %param.13) | copy-start | bytes 25165828
  135.9 31.2 %all-to-all-start.1 = ((bf16[8,4,16,1024]{3,2,1,0:T(8,128)(2,1)}), bf16[8,4,16,1024]{3,2,1,0:T(8,128)(2,1)S(1)}, u32[]{:S(2)}, u32[]{:S(2)}) async-start(bf16[8,4,16,1024]{3,2,1,0:T(8,128)(2,1)} %copy.29), calls=%async_computation.1 | async-start | bytes 2097152 | tf_op jit(solution)/shard_map/all_to_all | solution.py:59
  168.2 10.1 %copy-start.2 = (f32[1024]{0:T(1024)S(1)}, f32[1024]{0:T(1024)}, u32[]{:S(2)}) copy-start(f32[1024]{0:T(1024)} %param.10) | copy-start | bytes 12292
Sparse Core Ops, SparseCore 0:
  62.3 66.5 all-reduce.2
where the time goes:
time: 186 us
  waiting for transfers between devices  92.3 us (50%)
  blocking collectives  51.6 us (28%)
  matrix products  15.4 us (8%)
  between operations  13.5 us (7%)
  local copies, waits for them, and re-layouts  5.01 us (3%)
  starting transfers between devices  4.61 us (2%)
  other arithmetic  3.53 us (2%)
    psum x1, waiting for transfers between devices, run_experts(): lax.psum(up_part, 'tp').astype(jnp.float32)  66.7 us
    all_to_all x1, blocking collectives, on_device(): lax.all_to_all(outgoing, 'ep', split_axis=0, concat_axis=0, tiled=True)  31.2 us
    all_to_all x1, waiting for transfers between devices, on_device(): lax.all_to_all(answers, 'ep', split_axis=0, concat_axis=0, tiled=True)  25.6 us
    psum x1, blocking collectives, on_device(): sum_squares = lax.psum(jnp.sum(values * values, axis=1), 'tp')  11.4 us
    psum x1, blocking collectives, on_device(): out_squares = lax.psum(jnp.sum(combined * combined, axis=1), 'tp')  8.93 us
    dot_general x1, matrix products, run_experts(): jnp.einsum('secf,efd->secd', active, w_down, preferred_element_type=jnp.f...  5.89 us
    dot_general x1, matrix products, run_experts(): jnp.einsum('secd,edf->secf', slot_rows, w_up, preferred_element_type=jnp....  5.86 us
    all_to_all x1, starting transfers between devices, on_device(): lax.all_to_all(answers, 'ep', split_axis=0, concat_axis=0, tiled=True)  4.61 us
  transfers between devices with their start and end apart: 2, of which 2 were waited for; matrix products, arithmetic and copies ran while one was open for 1% of the time, Pallas kernels for 0%

commit v1 on v0

--- a/solution.py
+++ b/solution.py
@@ -32,7 +32,7 @@
     experts = local_experts * groups_ep
     capacity = max(2, 2 * tok_rows * top_count // experts)
     values = tokens.astype(jnp.float32)
-    sum_squares = lax.psum(jnp.sum(values * values, axis=1), "tp")
+    sum_squares = jnp.sum(lax.all_gather(jnp.sum(values * values, axis=1), "tp"), axis=0)
     normed = (values * lax.rsqrt(sum_squares / D + EPS)[:, None] * in_gain).astype(jnp.bfloat16)
     row_start = lax.axis_index("ep") * tok_rows
     my_routes = lax.dynamic_slice_in_dim(routes, row_start, tok_rows, 0)

time: 186 us -> 189 us (1.016)
    psum x1 -> x0, blocking collectives: 11.4 us -> none  [on_device(): sum_squares = lax.psum(jnp.sum(values * values, axis=1), 'tp')]
    unnamed x0 -> x1, blocking collectives: none -> 11.4 us
where the time goes in v1:
time: 189 us; the launch traced here: 188 us
  waiting for transfers between devices  92.3 us (49%)
  blocking collectives  51.5 us (27%)
  matrix products  15.5 us (8%)
  between operations  14.2 us (8%)
  local copies, waits for them, and re-layouts  6.59 us (3%)
  starting transfers between devices  4.61 us (2%)
  other arithmetic  3.55 us (2%)
    psum x1, waiting for transfers between devices, run_experts(): lax.psum(up_part, 'tp').astype(jnp.float32)  66.7 us
    all_to_all x1, blocking collectives, on_device(): lax.all_to_all(outgoing, 'ep', split_axis=0, concat_axis=0, tiled=True)  31.2 us
    all_to_all x1, waiting for transfers between devices, on_device(): lax.all_to_all(answers, 'ep', split_axis=0, concat_axis=0, tiled=True)  25.6 us
    unnamed x1, blocking collectives  11.4 us
    psum x1, blocking collectives, on_device(): out_squares = lax.psum(jnp.sum(combined * combined, axis=1), 'tp')  8.93 us
    dot_general x1, matrix products, run_experts(): jnp.einsum('secf,efd->secd', active, w_down, preferred_element_type=jnp.f...  5.9 us
    dot_general x1, matrix products, run_experts(): jnp.einsum('secd,edf->secf', slot_rows, w_up, preferred_element_type=jnp....  5.87 us
    all_to_all x1, starting transfers between devices, on_device(): lax.all_to_all(answers, 'ep', split_axis=0, concat_axis=0, tiled=True)  4.6 us
  transfers between devices with their start and end apart: 2, of which 2 were waited for; matrix products, arithmetic and copies ran while one was open for 1% of the time, Pallas kernels for 0%

profile of v1, /device:TPU:0, one launch (start us, length us, event | category | flops | bytes accessed | tf_op | source)
XLA Modules:
  0.0 188.2 jit_solution(4468226945776824936)
XLA Ops:
  6.5 0.0 copy-start
  6.5 0.0 all-reduce.4.cloned.1.call-start
  6.5 0.7 copy-done
  7.2 0.1 constant_dynamic-slice_fusion
  7.3 0.1 copy.33
  7.4 0.1 eq.42
  7.5 0.1 eq.38
  7.6 0.6 reduce-window.6
  8.2 0.2 slice_reduce_fusion
  8.5 0.1 fusion.42
  8.6 0.1 reduce_sum.50
  8.7 0.1 copy.26
  8.8 0.1 fusion.33
  8.9 1.0 fusion.34
  10.0 1.2 dynamic-slice
  11.9 0.2 dynamic-update-slice
  12.1 11.4 %all-reduce = f32[256]{0:T(256)S(1)} all-reduce(f32[256]{0:T(256)S(1)} %dynamic-update-slice), channel_id=2, replica_groups=mesh['ep'=8,'tp'=4] {'tp'}, use_global_device_ids=true, to_apply=%add | all-reduce | flops 256 | bytes 2048
  23.5 0.1 reshape.83
  23.6 1.4 convolution_convert_fusion
  25.0 31.2 %all_to_all.10 = bf16[8,4,16,1024]{3,2,1,0:T(8,128)(2,1)S(1)} all-to-all(bf16[8,4,16,1024]{3,2,1,0:T(8,128)(2,1)S(1)} %bitcast.59), channel_id=1, replica_groups=mesh['ep'=8,'tp'=4] {'ep'}, dimensions={0} | all-to-all | bytes 2097152 | tf_op jit(solution)/shard_map/all_to_all | solution.py:54
  56.3 0.0 copy-start.1
  56.3 5.9 %fusion.23 = bf16[8,4,16,1024]{3,2,0,1:T(8,128)(2,1)} fusion(bf16[4,1024,1024]{2,1,0:T(8,128)(2,1)} %param.14, bf16[8,4,16,1024]{3,2,1,0:T(8,128)(2,1)S(1)} %all_to_all.10), kind=kOutput, calls=%fused_computation.19 | convolution fusion | flops 1074266112 | bytes 10485760 | tf_op jit(solution)/shard_map/secd,edf->secf/dot_general | solution.py:14
  62.1 0.0 copy-done.1
  62.1 2.3 %fusion.26 = bf16[8,4,16,1024]{3,2,0,1:T(8,128)(2,1)} fusion(bf16[4,1024,1024]{2,1,0:T(8,128)(2,1)S(1)} %copy-done.1, bf16[8,4,16,1024]{3,2,1,0:T(8,128)(2,1)S(1)} %all_to_all.10), kind=kOutput, calls=%fused_computation.20 | convolution fusion | flops 1074266112 | bytes 10485760 | tf_op jit(solution)/shard_map/secd,edf->secf/dot_general | solution.py:11
  64.4 0.0 all-reduce.4.cloned.1.call-update
  64.4 66.7 %all-reduce.4.cloned.1.call-done = (bf16[8,4,16,1024]{3,2,0,1:T(8,128)(2,1)}, bf16[8,4,16,1024]{3,2,0,1:T(8,128)(2,1)}) async-done(((bf16[8,4,16,1024]{3,2,0,1:T(8,128)(2,1)}, bf16[8,4,16,1024]{3,2,0,1:T(8,128)(2,1)}), (bf16[8,4,16,1024]{3,2,0,1:T(8,128)(2,1)}, bf16[8,4,16,1024]{3,2,0,1:T(8,128)(2,1)})) %all-reduce.4.cloned.1.call-update) | async-done | bytes 2097168 | tf_op jit(solution)/shard_map/psum | solution.py:19
  131.1 5.9 %fusion.20 = bf16[8,4,16,1024]{3,2,0,1:T(8,128)(2,1)S(1)} fusion(bf16[4,1024,1024]{2,1,0:T(8,128)(2,1)} %param.15, bf16[8,4,16,1024]{3,2,0,1:T(8,128)(2,1)} %get-tuple-element.5, bf16[8,4,16,1024]{3,2,0,1:T(8,128)(2,1)} %get-tuple-element.6), kind=kOutput, calls=%fused_computation.18 | convolution fusion | flops 1078460416 | bytes 11534336 | tf_op jit(solution)/shard_map/secf,efd->secd/dot_general | solution.py:22
  137.0 1.1 copy.29
  138.1 4.6 %all-to-all-start.1 = ((bf16[8,4,16,1024]{3,2,1,0:T(8,128)(2,1)}), bf16[8,4,16,1024]{3,2,1,0:T(8,128)(2,1)S(1)}, u32[]{:S(2)}, u32[]{:S(2)}) async-start(bf16[8,4,16,1024]{3,2,1,0:T(8,128)(2,1)} %copy.29), calls=%async_computation.1 | async-start | bytes 2097152 | tf_op jit(solution)/shard_map/all_to_all | solution.py:59
  142.7 0.1 mul.89
  142.8 0.8 constant_dynamic-slice_fusion.1
  143.6 0.1 copy.23
  143.7 25.6 %all-to-all-done.1 = bf16[8,4,16,1024]{3,2,1,0:T(8,128)(2,1)S(1)} async-done(((bf16[8,4,16,1024]{3,2,1,0:T(8,128)(2,1)}), bf16[8,4,16,1024]{3,2,1,0:T(8,128)(2,1)S(1)}, u32[]{:S(2)}, u32[]{:S(2)}) %all-to-all-start.1) | async-done | bytes 1048608 | tf_op jit(solution)/shard_map/all_to_all | solution.py:59
  169.3 1.2 gather_fusion
  170.5 0.0 copy-start.2
  170.5 0.3 reshape.74
  170.8 0.7 multiply_reduce_fusion
  171.5 0.1 multiply_reduce_fusion.1
  171.6 8.9 %psum.23 = f32[64]{0:T(128)S(1)} all-reduce(f32[64]{0:T(128)S(1)} %multiply_reduce_fusion.1), channel_id=1, replica_groups=mesh['ep'=8,'tp'=4] {'tp'}, use_global_device_ids=true, to_apply=%region_10.11 | all-reduce | flops 64 | bytes 512 | tf_op jit(solution)/shard_map/psum | solution.py:63
  180.6 0.0 copy-done.2
  180.6 0.8 multiply_convert_fusion
  (10 shorter events, 0.1 us)
Async XLA Ops:
  6.5 0.7 copy-start
  6.5 124.6 %all-reduce.4.cloned.1.call-start = ((), (), s32[]{:S(2)}) async-start(), calls=%async_computation.2 | async-start | bytes 4194304 | tf_op jit(solution)/shard_map/psum | solution.py:19
  56.3 5.9 %copy-start.1 = (bf16[4,1024,1024]{2,1,0:T(8,128)(2,1)S(1)}, bf16[4,1024,1024]{2,1,0:T(8,128)(2,1)}, u32[]{:S(2)}) copy-start(bf16[4,1024,1024]{2,1,0:T(8,128)(2,1)} %param.13) | copy-start | bytes 25165828
  138.1 31.2 %all-to-all-start.1 = ((bf16[8,4,16,1024]{3,2,1,0:T(8,128)(2,1)}), bf16[8,4,16,1024]{3,2,1,0:T(8,128)(2,1)S(1)}, u32[]{:S(2)}, u32[]{:S(2)}) async-start(bf16[8,4,16,1024]{3,2,1,0:T(8,128)(2,1)} %copy.29), calls=%async_computation.1 | async-start | bytes 2097152 | tf_op jit(solution)/shard_map/all_to_all | solution.py:59
  170.5 10.1 %copy-start.2 = (f32[1024]{0:T(1024)S(1)}, f32[1024]{0:T(1024)}, u32[]{:S(2)}) copy-start(f32[1024]{0:T(1024)} %param.10) | copy-start | bytes 12292
Sparse Core Ops, SparseCore 0:
  64.5 66.5 all-reduce.3
